TPU v7x, 32 devices: a whole 2x2x4 slice. The times are simulated.
32 devices in a mesh: grp: 2 (over x), sp: 4 (over y, core), tp: 4 (over z).
Axes of the slice: x: 2, y: 2, z: 4, core: 2. Of those that a mesh axis runs over, the one named last changes fastest.
Arguments:
- tokens_in: bfloat16 [2048, 2048], P(('grp', 'sp'), 'tp'), parts along dimension 0, may hold values from -8 to 8
- out_gate: bfloat16 [3, 2048, 2048], P(None, 'sp', 'tp'), may hold values from -0.125 to 0.125
- in_gate: bfloat16 [3, 2048, 2048], P(None, 'sp', 'tp'), may hold values from -0.125 to 0.125
- value_proj: bfloat16 [3, 2048, 2048], P(None, 'sp', 'tp'), may hold values from -0.125 to 0.125
- mix_proj: bfloat16 [3, 2048, 2048], P(None, 'sp', 'tp'), may hold values from -0.125 to 0.125
- conv_taps: float32 [3, 3, 2048], P(None, None, 'tp'), may hold values from -3.5 to 3.5
- norm_gains: float32 [3, 2048], P(None, 'tp'), may hold values from 0.1 to 1.9
- final_gain: float32 [2048], P('tp'), may hold values from 0.1 to 1.9
Outputs:
- normed_out: bfloat16 [2048, 2048], P(('grp', 'sp'), 'tp'), parts along dimension 0
There are 2 independent parts, one for each index of `grp`. A program takes and returns all parts, laid end to end along the dimension named above; an argument that names none is the same for every part. Nothing has to cross between parts.
All inputs are finite; a program needn't handle non-finite values.
Results may differ from a plain program's by a relative error of at most 0.025.
Values may be sent and summed in bfloat16 or wider, within the bound.
A program may use at most 64 MiB of HBM per device.

v0:
```python
import jax
import jax.numpy as jnp
from jax import lax
from jax.sharding import PartitionSpec as P

D = 2048
TAPS = 3
LAYERS = 3
epsilon = 1e-06


def passed_along(shard, axis, by):
    peers = lax.axis_size(axis)
    pairs = [(i, i + by) for i in range(peers) if 0 <= i + by < peers]
    return lax.ppermute(shard, axis, pairs)


def row_scale(stream):
    squares = lax.psum(jnp.sum(stream * stream, axis=1, keepdims=True), "tp")
    return lax.rsqrt(squares / D + epsilon)


def shards(tokens_in, out_gate, in_gate, value_proj, mix_proj, conv_taps, norm_gains, final_gain):
    stream = tokens_in.astype(jnp.float32)
    row_count = stream.shape[0]
    reach = TAPS - 1
    whole = (
        lax.all_gather(out_gate, "sp", axis=1, tiled=True),
        lax.all_gather(in_gate, "sp", axis=1, tiled=True),
        lax.all_gather(value_proj, "sp", axis=1, tiled=True),
        lax.all_gather(mix_proj, "sp", axis=1, tiled=True),
    )
    for layer_index in range(LAYERS):
        scale = row_scale(stream)
        normed = (stream * norm_gains[layer_index]).astype(jnp.bfloat16)
        gathered = lax.all_gather(normed, "tp", axis=1, tiled=True)
        products = tuple(
            (
                jnp.dot(gathered, weight[layer_index], preferred_element_type=jnp.float32)
                for weight in whole[:3]
            )
        )
        out_gates, in_gates, values = [
            (product * scale).astype(jnp.bfloat16) for product in products
        ]
        product_v = (in_gates.astype(jnp.float32) * values.astype(jnp.float32)).astype(jnp.bfloat16)
        earlier = passed_along(product_v[row_count - reach :], "sp", 1)
        padded = jnp.concatenate([earlier, product_v], axis=0)
        convolved = padded[0:row_count].astype(jnp.float32) * conv_taps[layer_index, 0]
        for tap_index in range(1, TAPS):
            convolved = (
                convolved
                + padded[tap_index : tap_index + row_count].astype(jnp.float32)
                * conv_taps[layer_index, tap_index]
            )
        gated = (out_gates.astype(jnp.float32) * convolved).astype(jnp.bfloat16)
        spread = lax.all_gather(gated, "tp", axis=1, tiled=True)
        mixed = jnp.dot(spread, whole[3][layer_index], preferred_element_type=jnp.float32)
        stream = stream + mixed
    scale = row_scale(stream)
    return (stream * scale * final_gain).astype(jnp.bfloat16)


def solution(mesh):
    in_specs = (
        P(("grp", "sp"), "tp"),
        P(None, "sp", "tp"),
        P(None, "sp", "tp"),
        P(None, "sp", "tp"),
        P(None, "sp", "tp"),
        P(None, None, "tp"),
        P(None, "tp"),
        P("tp"),
    )
    out_specs = P(("grp", "sp"), "tp")
    return jax.shard_map(shards, mesh=mesh, in_specs=in_specs, out_specs=out_specs, check_vma=False)
```

profile of v0, /device:TPU:0, one launch (start us, length us, event | category | flops | bytes accessed | tf_op | source)
XLA Modules:
  0.0 424.5 jit_solution(9574232206159354128)
XLA Ops:
  6.5 0.8 fusion.60
  7.4 1.7 fusion.55
  11.8 13.5 %psum.28 = f32[256,1]{0,1:T(1,128)S(1)} all-reduce(f32[256,1]{0,1:T(1,128)S(1)} %bitcast.159), channel_id=1, replica_groups=mesh['grp'=2,'sp'=4,'tp'=4] {'tp'}, use_global_device_ids=true, to_apply=%region_1.0 | all-reduce | flops 256 | bytes 2048 | tf_op jit(solution)/shard_map/psum | solution.py:19
  25.3 14.7 %all-gather.11.cloned.1.call-done = bf16[256,2048]{1,0:T(8,128)(2,1)} async-done(((bf16[256,512]{1,0:T(8,128)(2,1)}), bf16[256,2048]{1,0:T(8,128)(2,1)}) %all-gather.11.cloned.1.call-update) | async-done | bytes 1048592 | tf_op jit(solution)/shard_map/all_gather | solution.py:36
  40.0 47.3 %all-gather.17.cloned.1.call-done = bf16[3,2048,512]{2,1,0:T(8,128)(2,1)} async-done(((bf16[3,512,512]{2,1,0:T(8,128)(2,1)}), bf16[3,2048,512]{2,1,0:T(8,128)(2,1)}) %all-gather.17.cloned.1.call-update) | async-done | bytes 6291472 | tf_op jit(solution)/shard_map/all_gather | solution.py:30
  87.3 2.6 fusion.39
  90.0 45.3 %all-gather.15.cloned.1.call-done = bf16[3,2048,512]{2,1,0:T(8,128)(2,1)} async-done(((bf16[3,512,512]{2,1,0:T(8,128)(2,1)}), bf16[3,2048,512]{2,1,0:T(8,128)(2,1)}) %all-gather.15.cloned.1.call-update) | async-done | bytes 6291472 | tf_op jit(solution)/shard_map/all_gather | solution.py:29
  135.3 2.6 fusion.38
  137.9 2.2 collective-permute-start
  140.1 43.0 %all-gather.13.cloned.1.call-done = bf16[3,2048,512]{2,1,0:T(8,128)(2,1)} async-done(((bf16[3,512,512]{2,1,0:T(8,128)(2,1)}), bf16[3,2048,512]{2,1,0:T(8,128)(2,1)}) %all-gather.13.cloned.1.call-update) | async-done | bytes 6291472 | tf_op jit(solution)/shard_map/all_gather | solution.py:28
  183.1 3.1 fusion.35
  186.3 44.6 %all-gather.21.cloned.1.call-done = bf16[3,2048,512]{2,1,0:T(8,128)(2,1)} async-done(((bf16[3,512,512]{2,1,0:T(8,128)(2,1)}), bf16[3,2048,512]{2,1,0:T(8,128)(2,1)}) %all-gather.21.cloned.1.call-update) | async-done | bytes 6291472 | tf_op jit(solution)/shard_map/all_gather | solution.py:31
  230.9 29.4 %all-gather.19.cloned.1.call-done = bf16[256,2048]{1,0:T(8,128)(2,1)} async-done(((bf16[256,512]{1,0:T(8,128)(2,1)}), bf16[256,2048]{1,0:T(8,128)(2,1)}) %all-gather.19.cloned.1.call-update) | async-done | bytes 1048592 | tf_op jit(solution)/shard_map/all_gather | solution.py:57
  260.3 3.4 multiply_reduce_fusion.2
  263.8 10.3 %psum.29 = f32[256,1]{0,1:T(1,128)S(1)} all-reduce(f32[256,1]{0,1:T(1,128)S(1)} %bitcast.182), channel_id=1, replica_groups=mesh['grp'=2,'sp'=4,'tp'=4] {'tp'}, use_global_device_ids=true, to_apply=%region_3.0 | all-reduce | flops 256 | bytes 2048 | tf_op jit(solution)/shard_map/psum | solution.py:19
  274.1 17.2 %all-gather.23.cloned.1.call-done = bf16[256,2048]{1,0:T(8,128)(2,1)} async-done(((bf16[256,512]{1,0:T(8,128)(2,1)}), bf16[256,2048]{1,0:T(8,128)(2,1)}) %all-gather.23.cloned.1.call-update) | async-done | bytes 1048592 | tf_op jit(solution)/shard_map/all_gather | solution.py:36
  291.2 2.7 fusion.46
  293.9 2.6 fusion.45
  296.6 1.3 collective-permute-start.1
  298.7 3.1 fusion.42
  301.9 30.3 %all-gather.25.cloned.1.call-done = bf16[256,2048]{1,0:T(8,128)(2,1)} async-done(((bf16[256,512]{1,0:T(8,128)(2,1)}), bf16[256,2048]{1,0:T(8,128)(2,1)}) %all-gather.25.cloned.1.call-update) | async-done | bytes 1048592 | tf_op jit(solution)/shard_map/all_gather | solution.py:57
  332.2 3.3 multiply_reduce_fusion.1
  335.6 10.3 %psum.30 = f32[256,1]{0,1:T(1,128)S(1)} all-reduce(f32[256,1]{0,1:T(1,128)S(1)} %bitcast.181), channel_id=1, replica_groups=mesh['grp'=2,'sp'=4,'tp'=4] {'tp'}, use_global_device_ids=true, to_apply=%region_5.0 | all-reduce | flops 256 | bytes 2048 | tf_op jit(solution)/shard_map/psum | solution.py:19
  345.9 17.2 %all-gather.27.cloned.1.call-done = bf16[256,2048]{1,0:T(8,128)(2,1)} async-done(((bf16[256,512]{1,0:T(8,128)(2,1)}), bf16[256,2048]{1,0:T(8,128)(2,1)}) %all-gather.27.cloned.1.call-update) | async-done | bytes 1048592 | tf_op jit(solution)/shard_map/all_gather | solution.py:36
  363.0 2.7 fusion.53
  365.7 2.6 fusion.52
  368.4 1.3 collective-permute-start.2
  370.5 3.1 fusion.49
  373.6 30.3 %all-gather.29.cloned.1.call-done = bf16[256,2048]{1,0:T(8,128)(2,1)} async-done(((bf16[256,512]{1,0:T(8,128)(2,1)}), bf16[256,2048]{1,0:T(8,128)(2,1)}) %all-gather.29.cloned.1.call-update) | async-done | bytes 1048592 | tf_op jit(solution)/shard_map/all_gather | solution.py:57
  404.0 2.7 multiply_reduce_fusion
  406.7 10.2 %psum.31 = f32[256,1]{0,1:T(1,128)S(1)} all-reduce(f32[256,1]{0,1:T(1,128)S(1)} %bitcast.183), channel_id=1, replica_groups=mesh['grp'=2,'sp'=4,'tp'=4] {'tp'}, use_global_device_ids=true, to_apply=%region_7.0 | all-reduce | flops 256 | bytes 2048 | tf_op jit(solution)/shard_map/psum | solution.py:19
  416.8 0.8 multiply_convert_fusion
  (43 shorter events, 4.6 us)
Async XLA Ops:
  6.5 33.5 %all-gather.11.cloned.1.call-start = ((), (), s32[]{:S(2)}) async-start(), calls=%async_computation | async-start | bytes 1310720 | tf_op jit(solution)/shard_map/all_gather | solution.py:36
  9.1 78.2 %all-gather.17.cloned.1.call-start = ((), (), s32[]{:S(2)}) async-start(), calls=%async_computation.3 | async-start | bytes 7864320 | tf_op jit(solution)/shard_map/all_gather | solution.py:30
  9.9 125.4 %all-gather.15.cloned.1.call-start = ((), (), s32[]{:S(2)}) async-start(), calls=%async_computation.2 | async-start | bytes 7864320 | tf_op jit(solution)/shard_map/all_gather | solution.py:29
  10.6 129.5 %copy-start.1 = (f32[3,3,512]{2,1,0:T(4,128)S(1)}, f32[3,3,512]{2,1,0:T(4,128)}, u32[]{:S(2)}) copy-start(f32[3,3,512]{2,1,0:T(4,128)} %param.13) | copy-start | bytes 55300
  10.6 172.5 %all-gather.13.cloned.1.call-start = ((), (), s32[]{:S(2)}) async-start(), calls=%async_computation.1 | async-start | bytes 7864320 | tf_op jit(solution)/shard_map/all_gather | solution.py:28
  11.2 219.7 %all-gather.21.cloned.1.call-start = ((), (), s32[]{:S(2)}) async-start(), calls=%async_computation.5 | async-start | bytes 7864320 | tf_op jit(solution)/shard_map/all_gather | solution.py:31
  11.8 248.6 %all-gather.19.cloned.1.call-start = ((), (), s32[]{:S(2)}) async-start(), calls=%async_computation.4 | async-start | bytes 1310720 | tf_op jit(solution)/shard_map/all_gather | solution.py:57
  40.0 143.1 %copy-start.3 = (bf16[256,2048]{1,0:T(8,128)(2,1)S(1)}, bf16[256,2048]{1,0:T(8,128)(2,1)}, u32[]{:S(2)}) copy-start(bf16[256,2048]{1,0:T(8,128)(2,1)} %all-gather.11.cloned.1.call-done) | copy-start | bytes 3145732
  90.0 170.4 %copy-start = (bf16[256,512]{1,0:T(8,128)(2,1)S(1)}, bf16[256,512]{1,0:T(8,128)(2,1)}, u32[]{:S(2)}) copy-start(bf16[256,512]{1,0:T(8,128)(2,1)} %param.8) | copy-start | bytes 786436
  137.9 45.2 %collective-permute-start = (bf16[2,512]{1,0:T(2,128)(2,1)S(1)}, bf16[2,512]{1,0:T(2,128)(2,1)S(1)}, u32[]{:S(2)}, u32[]{:S(2)}) collective-permute-start(bf16[2,512]{1,0:T(2,128)(2,1)S(1)} %slice.135), channel_id=1, source_target_pairs={{0,4},{4,8},{8,12},{1,5},{5,9},{9,13},{2,6},{6,10},{10,14},{3,7},{... | collective-permute-start | bytes 6152 | tf_op jit(solution)/shard_map/ppermute | solution.py:15
  186.2 105.0 %all-gather.23.cloned.1.call-start = ((), (), s32[]{:S(2)}) async-start(), calls=%async_computation.6 | async-start | bytes 1310720 | tf_op jit(solution)/shard_map/all_gather | solution.py:36
  263.7 68.4 %all-gather.25.cloned.1.call-start = ((), (), s32[]{:S(2)}) async-start(), calls=%async_computation.7 | async-start | bytes 1310720 | tf_op jit(solution)/shard_map/all_gather | solution.py:57
  291.2 7.5 %copy-start.5 = (bf16[256,2048]{1,0:T(8,128)(2,1)S(1)}, bf16[256,2048]{1,0:T(8,128)(2,1)}, u32[]{:S(2)}) copy-start(bf16[256,2048]{1,0:T(8,128)(2,1)} %all-gather.23.cloned.1.call-done) | copy-start | bytes 3145732
  296.6 2.1 collective-permute-start.1
  301.8 61.2 %all-gather.27.cloned.1.call-start = ((), (), s32[]{:S(2)}) async-start(), calls=%async_computation.8 | async-start | bytes 1310720 | tf_op jit(solution)/shard_map/all_gather | solution.py:36
  335.5 68.4 %all-gather.29.cloned.1.call-start = ((), (), s32[]{:S(2)}) async-start(), calls=%async_computation.9 | async-start | bytes 1310720 | tf_op jit(solution)/shard_map/all_gather | solution.py:57
  363.0 7.5 %copy-start.4 = (bf16[256,2048]{1,0:T(8,128)(2,1)S(1)}, bf16[256,2048]{1,0:T(8,128)(2,1)}, u32[]{:S(2)}) copy-start(bf16[256,2048]{1,0:T(8,128)(2,1)} %all-gather.27.cloned.1.call-done) | copy-start | bytes 3145732
  368.4 48.5 %copy-start.2 = (f32[512]{0:T(512)S(1)}, f32[512]{0:T(512)}, u32[]{:S(2)}) copy-start(f32[512]{0:T(512)} %param.15) | copy-start | bytes 6148
  368.4 2.1 collective-permute-start.2
Sparse Core Ops, SparseCore 0:
  9.2 30.7 all-gather.10
  41.6 45.7 all-gather.16
  88.9 46.3 all-gather.14
  136.7 46.3 all-gather.12
  184.5 46.3 all-gather.20
  232.3 27.9 all-gather.18
  263.8 27.3 all-gather.22
  302.0 30.1 all-gather.24
  335.6 27.3 all-gather.26
  373.8 30.1 all-gather.28
where the time goes:
time: 425 us
  waiting for transfers between devices  323 us (76%)
  blocking collectives  44.2 us (10%)
  matrix products  34.6 us (8%)
  between operations  13.7 us (3%)
  starting transfers between devices  5.1 us (1%)
    all_gather x3, waiting for transfers between devices, shards(): spread = lax.all_gather(gated, 'tp', axis=1, tiled=True)  90 us
    all_gather x3, waiting for transfers between devices, shards(): gathered = lax.all_gather(normed, 'tp', axis=1, tiled=True)  49.1 us
    all_gather x1, waiting for transfers between devices, shards(): lax.all_gather(value_proj, 'sp', axis=1, tiled=True)  47.3 us
    all_gather x1, waiting for transfers between devices, shards(): lax.all_gather(in_gate, 'sp', axis=1, tiled=True)  45.3 us
    all_gather x1, waiting for transfers between devices, shards(): lax.all_gather(mix_proj, 'sp', axis=1, tiled=True)  44.6 us
    psum x4, blocking collectives, row_scale(): squares = lax.psum(jnp.sum(stream * stream, axis=1, keepdims=True), 'tp')  44.2 us
    all_gather x1, waiting for transfers between devices, shards(): lax.all_gather(out_gate, 'sp', axis=1, tiled=True)  43 us
    dot_general x9, matrix products, shards(): jnp.dot(gathered, weight[layer_index], preferred_element_type=jnp.float32)  25.2 us
  transfers between devices with their start and end apart: 13, of which 12 were waited for; matrix products, arithmetic and copies ran while one was open for 2% of the time, Pallas kernels for 0%

commit v1 on v0

--- a/solution.py
+++ b/solution.py
@@ -7,6 +7,19 @@
 TAPS = 3
 LAYERS = 3
 epsilon = 1e-06
+
+
+def register_ranges(inner_x, device_axis, k_dim):
+    size_here = jax.lax.axis_size(device_axis)
+    heap = tuple(((k0, (k0 + 1) % size_here) for k0 in range(size_here)))
+
+    def clear_vector(even):
+        if len(even) == size_here:
+            return even
+        return clear_vector([jax.lax.ppermute(even[0], device_axis, heap), *even])
+
+    fresh = jnp.concatenate(clear_vector([inner_x]), k_dim)
+    return jnp.roll(fresh, (jax.lax.axis_index(device_axis) + 1) * inner_x.shape[k_dim], k_dim)
 
 
 def passed_along(shard, axis, by):
@@ -54,7 +67,7 @@
                 * conv_taps[layer_index, tap_index]
             )
         gated = (out_gates.astype(jnp.float32) * convolved).astype(jnp.bfloat16)
-        spread = lax.all_gather(gated, "tp", axis=1, tiled=True)
+        spread = register_ranges(gated, "tp", 1)
         mixed = jnp.dot(spread, whole[3][layer_index], preferred_element_type=jnp.float32)
         stream = stream + mixed
     scale = row_scale(stream)

time: 425 us -> 393 us (0.925)
  waiting for transfers between devices: 323 us -> 291 us
  starting transfers between devices: 5.1 us -> 9.44 us
    all_gather x3 -> x0, waiting for transfers between devices: 90 us -> none  [shards(): spread = lax.all_gather(gated, 'tp', axis=1, tiled=True)]
    ppermute x0 -> x9, waiting for transfers between devices: none -> 77.1 us  [clear_vector(): return clear_vector([jax.lax.ppermute(even[0], device_axis, heap), *even])]
    all_gather x1, waiting for transfers between devices: 44.6 us -> 25.7 us  [shards(): lax.all_gather(mix_proj, 'sp', axis=1, tiled=True)]
    ppermute x0 -> x9, starting transfers between devices: none -> 4.44 us  [clear_vector(): return clear_vector([jax.lax.ppermute(even[0], device_axis, heap), *even])]
  transfers between devices with their start and end apart: 13 -> 19, of which waited for: 12 -> 17; matrix products, arithmetic and copies ran while one was open for 2% -> 2% of each run, Pallas kernels for 0% -> 0%
where the time goes in v1:
time: 393 us
  waiting for transfers between devices  291 us (74%)
  blocking collectives  42.3 us (11%)
  matrix products  33.3 us (8%)
  between operations  13.6 us (3%)
  starting transfers between devices  9.44 us (2%)
    ppermute x9, waiting for transfers between devices, clear_vector(): return clear_vector([jax.lax.ppermute(even[0], device_axis, heap), *even])  77.1 us
    all_gather x3, waiting for transfers between devices, shards(): gathered = lax.all_gather(normed, 'tp', axis=1, tiled=True)  47.8 us
    all_gather x1, waiting for transfers between devices, shards(): lax.all_gather(value_proj, 'sp', axis=1, tiled=True)  47.3 us
    all_gather x1, waiting for transfers between devices, shards(): lax.all_gather(in_gate, 'sp', axis=1, tiled=True)  45.2 us
    all_gather x1, waiting for transfers between devices, shards(): lax.all_gather(out_gate, 'sp', axis=1, tiled=True)  43.3 us
    psum x4, blocking collectives, row_scale(): squares = lax.psum(jnp.sum(stream * stream, axis=1, keepdims=True), 'tp')  42.3 us
    all_gather x1, waiting for transfers between devices, shards(): lax.all_gather(mix_proj, 'sp', axis=1, tiled=True)  25.7 us
    dot_general x9, matrix products, shards(): jnp.dot(gathered, weight[layer_index], preferred_element_type=jnp.float32)  22.3 us
  transfers between devices with their start and end apart: 19, of which 17 were waited for; matrix products, arithmetic and copies ran while one was open for 2% of the time, Pallas kernels for 0%

profile of v1, /device:TPU:0, one launch (start us, length us, event | category | flops | bytes accessed | tf_op | source)
XLA Modules:
  0.0 392.7 jit_solution(13088888377769784734)
XLA Ops:
  11.8 13.5 %psum.28 = f32[256,1]{0,1:T(1,128)S(1)} all-reduce(f32[256,1]{0,1:T(1,128)S(1)} %bitcast.156), channel_id=1, replica_groups=mesh['grp'=2,'sp'=4,'tp'=4] {'tp'}, use_global_device_ids=true, to_apply=%region_1.0 | all-reduce | flops 256 | bytes 2048 | tf_op jit(solution)/shard_map/psum | solution.py:32
  25.3 14.7 %all-gather.8.cloned.1.call-done = bf16[256,2048]{1,0:T(8,128)(2,1)} async-done(((bf16[256,512]{1,0:T(8,128)(2,1)}), bf16[256,2048]{1,0:T(8,128)(2,1)}) %all-gather.8.cloned.1.call-update) | async-done | bytes 1048592 | tf_op jit(solution)/shard_map/all_gather | solution.py:49
  40.0 47.3 %all-gather.14.cloned.1.call-done = bf16[3,2048,512]{2,1,0:T(8,128)(2,1)} async-done(((bf16[3,512,512]{2,1,0:T(8,128)(2,1)}), bf16[3,2048,512]{2,1,0:T(8,128)(2,1)}) %all-gather.14.cloned.1.call-update) | async-done | bytes 6291472 | tf_op jit(solution)/shard_map/all_gather | solution.py:43
  87.3 2.7 fusion.39
  90.1 45.2 %all-gather.12.cloned.1.call-done = bf16[3,2048,512]{2,1,0:T(8,128)(2,1)} async-done(((bf16[3,512,512]{2,1,0:T(8,128)(2,1)}), bf16[3,2048,512]{2,1,0:T(8,128)(2,1)}) %all-gather.12.cloned.1.call-update) | async-done | bytes 6291472 | tf_op jit(solution)/shard_map/all_gather | solution.py:42
  135.3 2.3 fusion.38
  137.6 2.2 collective-permute-start
  139.8 43.3 %all-gather.10.cloned.1.call-done = bf16[3,2048,512]{2,1,0:T(8,128)(2,1)} async-done(((bf16[3,512,512]{2,1,0:T(8,128)(2,1)}), bf16[3,2048,512]{2,1,0:T(8,128)(2,1)}) %all-gather.10.cloned.1.call-update) | async-done | bytes 6291472 | tf_op jit(solution)/shard_map/all_gather | solution.py:41
  183.1 2.4 fusion.35
  187.1 8.8 %collective-permute-done.1 = bf16[256,512]{1,0:T(8,128)(2,1)S(1)} collective-permute-done((bf16[256,512]{1,0:T(8,128)(2,1)S(1)}, bf16[256,512]{1,0:T(8,128)(2,1)S(1)}, u32[]{:S(2)}, u32[]{:S(2)}) %collective-permute-start.1) | collective-permute-done | bytes 262176 | tf_op jit(solution)/shard_map/ppermute | solution.py:19
  195.9 9.4 %collective-permute-done.2 = bf16[256,512]{1,0:T(8,128)(2,1)S(1)} collective-permute-done((bf16[256,512]{1,0:T(8,128)(2,1)S(1)}, bf16[256,512]{1,0:T(8,128)(2,1)S(1)}, u32[]{:S(2)}, u32[]{:S(2)}) %collective-permute-start.2) | collective-permute-done | bytes 262176 | tf_op jit(solution)/shard_map/ppermute | solution.py:19
  205.3 25.7 %all-gather.16.cloned.1.call-done = bf16[3,2048,512]{2,1,0:T(8,128)(2,1)} async-done(((bf16[3,512,512]{2,1,0:T(8,128)(2,1)}), bf16[3,2048,512]{2,1,0:T(8,128)(2,1)}) %all-gather.16.cloned.1.call-update) | async-done | bytes 6291472 | tf_op jit(solution)/shard_map/all_gather | solution.py:44
  230.9 3.9 multiply_reduce_fusion.2
  234.9 11.9 %psum.29 = f32[256,1]{0,1:T(1,128)S(1)} all-reduce(f32[256,1]{0,1:T(1,128)S(1)} %bitcast.178), channel_id=1, replica_groups=mesh['grp'=2,'sp'=4,'tp'=4] {'tp'}, use_global_device_ids=true, to_apply=%region_3.5 | all-reduce | flops 256 | bytes 2048 | tf_op jit(solution)/shard_map/psum | solution.py:32
  246.8 16.3 %all-gather.18.cloned.1.call-done = bf16[256,2048]{1,0:T(8,128)(2,1)} async-done(((bf16[256,512]{1,0:T(8,128)(2,1)}), bf16[256,2048]{1,0:T(8,128)(2,1)}) %all-gather.18.cloned.1.call-update) | async-done | bytes 1048592 | tf_op jit(solution)/shard_map/all_gather | solution.py:49
  263.1 2.7 fusion.46
  265.8 2.3 fusion.45
  270.2 2.4 fusion.42
  274.0 8.6 %collective-permute-done.5 = bf16[256,512]{1,0:T(8,128)(2,1)S(1)} collective-permute-done((bf16[256,512]{1,0:T(8,128)(2,1)S(1)}, bf16[256,512]{1,0:T(8,128)(2,1)S(1)}, u32[]{:S(2)}, u32[]{:S(2)}) %collective-permute-start.5) | collective-permute-done | bytes 262176 | tf_op jit(solution)/shard_map/ppermute | solution.py:19
  282.7 10.9 %collective-permute-done.6 = bf16[256,512]{1,0:T(8,128)(2,1)S(1)} collective-permute-done((bf16[256,512]{1,0:T(8,128)(2,1)S(1)}, bf16[256,512]{1,0:T(8,128)(2,1)S(1)}, u32[]{:S(2)}, u32[]{:S(2)}) %collective-permute-start.6) | collective-permute-done | bytes 262176 | tf_op jit(solution)/shard_map/ppermute | solution.py:19
  293.5 10.0 %collective-permute-done.7 = bf16[256,512]{1,0:T(8,128)(2,1)S(1)} collective-permute-done((bf16[256,512]{1,0:T(8,128)(2,1)S(1)}, bf16[256,512]{1,0:T(8,128)(2,1)S(1)}, u32[]{:S(2)}, u32[]{:S(2)}) %collective-permute-start.7) | collective-permute-done | bytes 262176 | tf_op jit(solution)/shard_map/ppermute | solution.py:19
  303.5 3.9 multiply_reduce_fusion.1
  307.4 8.5 %psum.30 = f32[256,1]{0,1:T(1,128)S(1)} all-reduce(f32[256,1]{0,1:T(1,128)S(1)} %bitcast.179), channel_id=1, replica_groups=mesh['grp'=2,'sp'=4,'tp'=4] {'tp'}, use_global_device_ids=true, to_apply=%region_5.7 | all-reduce | flops 256 | bytes 2048 | tf_op jit(solution)/shard_map/psum | solution.py:32
  315.9 16.9 %all-gather.20.cloned.1.call-done = bf16[256,2048]{1,0:T(8,128)(2,1)} async-done(((bf16[256,512]{1,0:T(8,128)(2,1)}), bf16[256,2048]{1,0:T(8,128)(2,1)}) %all-gather.20.cloned.1.call-update) | async-done | bytes 1048592 | tf_op jit(solution)/shard_map/all_gather | solution.py:49
  332.8 2.7 fusion.53
  335.5 2.3 fusion.52
  340.0 2.4 fusion.49
  343.9 8.4 %collective-permute-done.9 = bf16[256,512]{1,0:T(8,128)(2,1)S(1)} collective-permute-done((bf16[256,512]{1,0:T(8,128)(2,1)S(1)}, bf16[256,512]{1,0:T(8,128)(2,1)S(1)}, u32[]{:S(2)}, u32[]{:S(2)}) %collective-permute-start.9) | collective-permute-done | bytes 262176 | tf_op jit(solution)/shard_map/ppermute | solution.py:19
  352.3 11.0 %collective-permute-done.10 = bf16[256,512]{1,0:T(8,128)(2,1)S(1)} collective-permute-done((bf16[256,512]{1,0:T(8,128)(2,1)S(1)}, bf16[256,512]{1,0:T(8,128)(2,1)S(1)}, u32[]{:S(2)}, u32[]{:S(2)}) %collective-permute-start.10) | collective-permute-done | bytes 262176 | tf_op jit(solution)/shard_map/ppermute | solution.py:19
  363.2 10.1 %collective-permute-done.11 = bf16[256,512]{1,0:T(8,128)(2,1)S(1)} collective-permute-done((bf16[256,512]{1,0:T(8,128)(2,1)S(1)}, bf16[256,512]{1,0:T(8,128)(2,1)S(1)}, u32[]{:S(2)}, u32[]{:S(2)}) %collective-permute-start.11) | collective-permute-done | bytes 262176 | tf_op jit(solution)/shard_map/ppermute | solution.py:19
  373.4 3.3 multiply_reduce_fusion
  376.6 8.4 %psum.31 = f32[256,1]{0,1:T(1,128)S(1)} all-reduce(f32[256,1]{0,1:T(1,128)S(1)} %bitcast.180), channel_id=1, replica_groups=mesh['grp'=2,'sp'=4,'tp'=4] {'tp'}, use_global_device_ids=true, to_apply=%region_7.9 | all-reduce | flops 256 | bytes 2048 | tf_op jit(solution)/shard_map/psum | solution.py:32
  (52 shorter events, 14.8 us)
Async XLA Ops:
  6.5 33.5 %all-gather.8.cloned.1.call-start = ((), (), s32[]{:S(2)}) async-start(), calls=%async_computation | async-start | bytes 1310720 | tf_op jit(solution)/shard_map/all_gather | solution.py:49
  9.1 78.2 %all-gather.14.cloned.1.call-start = ((), (), s32[]{:S(2)}) async-start(), calls=%async_computation.3 | async-start | bytes 7864320 | tf_op jit(solution)/shard_map/all_gather | solution.py:43
  9.9 125.4 %all-gather.12.cloned.1.call-start = ((), (), s32[]{:S(2)}) async-start(), calls=%async_computation.2 | async-start | bytes 7864320 | tf_op jit(solution)/shard_map/all_gather | solution.py:42
  10.6 172.5 %all-gather.10.cloned.1.call-start = ((), (), s32[]{:S(2)}) async-start(), calls=%async_computation.1 | async-start | bytes 7864320 | tf_op jit(solution)/shard_map/all_gather | solution.py:41
  11.2 219.7 %all-gather.16.cloned.1.call-start = ((), (), s32[]{:S(2)}) async-start(), calls=%async_computation.4 | async-start | bytes 7864320 | tf_op jit(solution)/shard_map/all_gather | solution.py:44
  11.8 251.3 %all-gather.18.cloned.1.call-start = ((), (), s32[]{:S(2)}) async-start(), calls=%async_computation.5 | async-start | bytes 1310720 | tf_op jit(solution)/shard_map/all_gather | solution.py:49
  87.3 48.0 %copy-start.3 = (bf16[256,2048]{1,0:T(8,128)(2,1)S(1)}, bf16[256,2048]{1,0:T(8,128)(2,1)}, u32[]{:S(2)}) copy-start(bf16[256,2048]{1,0:T(8,128)(2,1)} %all-gather.8.cloned.1.call-done) | copy-start | bytes 3145732
  90.0 49.7 %copy-start.1 = (f32[3,3,512]{2,1,0:T(4,128)S(1)}, f32[3,3,512]{2,1,0:T(4,128)}, u32[]{:S(2)}) copy-start(f32[3,3,512]{2,1,0:T(4,128)} %param.15) | copy-start | bytes 55300
  137.6 45.5 %collective-permute-start = (bf16[2,512]{1,0:T(2,128)(2,1)S(1)}, bf16[2,512]{1,0:T(2,128)(2,1)S(1)}, u32[]{:S(2)}, u32[]{:S(2)}) collective-permute-start(bf16[2,512]{1,0:T(2,128)(2,1)S(1)} %slice.135), channel_id=1, source_target_pairs={{0,4},{4,8},{8,12},{1,5},{5,9},{9,13},{2,6},{6,10},{10,14},{3,7},{... | collective-permute-start | bytes 6152 | tf_op jit(solution)/shard_map/ppermute | solution.py:28
  183.1 47.8 %copy-start = (bf16[256,512]{1,0:T(8,128)(2,1)S(1)}, bf16[256,512]{1,0:T(8,128)(2,1)}, u32[]{:S(2)}) copy-start(bf16[256,512]{1,0:T(8,128)(2,1)} %param.10) | copy-start | bytes 786436
  185.5 10.3 %collective-permute-start.1 = (bf16[256,512]{1,0:T(8,128)(2,1)S(1)}, bf16[256,512]{1,0:T(8,128)(2,1)S(1)}, u32[]{:S(2)}, u32[]{:S(2)}) collective-permute-start(bf16[256,512]{1,0:T(8,128)(2,1)S(1)} %fusion.35), channel_id=1, source_target_pairs={{0,1},{1,2},{2,3},{3,0},{4,5},{5,6},{6,7},{7,4},{8,9},{9,10},{10,1... | collective-permute-start | bytes 786440 | tf_op jit(solution)/shard_map/ppermute | solution.py:19
  195.9 9.4 %collective-permute-start.2 = (bf16[256,512]{1,0:T(8,128)(2,1)S(1)}, bf16[256,512]{1,0:T(8,128)(2,1)S(1)}, u32[]{:S(2)}, u32[]{:S(2)}) collective-permute-start(bf16[256,512]{1,0:T(8,128)(2,1)S(1)} %collective-permute-done.1), channel_id=1, source_target_pairs={{0,1},{1,2},{2,3},{3,0},{4,5},{5,6},{6,7},{7,4},{8,9},{9,10},{10,1... | collective-permute-start | bytes 786440 | tf_op jit(solution)/shard_map/ppermute | solution.py:19
  205.3 25.7 %collective-permute-start.3 = (bf16[256,512]{1,0:T(8,128)(2,1)S(1)}, bf16[256,512]{1,0:T(8,128)(2,1)S(1)}, u32[]{:S(2)}, u32[]{:S(2)}) collective-permute-start(bf16[256,512]{1,0:T(8,128)(2,1)S(1)} %collective-permute-done.2), channel_id=1, source_target_pairs={{0,1},{1,2},{2,3},{3,0},{4,5},{5,6},{6,7},{7,4},{8,9},{9,10},{10,1... | collective-permute-start | bytes 786440 | tf_op jit(solution)/shard_map/ppermute | solution.py:19
  234.8 98.0 %all-gather.20.cloned.1.call-start = ((), (), s32[]{:S(2)}) async-start(), calls=%async_computation.6 | async-start | bytes 1310720 | tf_op jit(solution)/shard_map/all_gather | solution.py:49
  263.1 2.7 copy-start.5
  268.1 2.1 collective-permute-start.4
  272.7 10.0 %collective-permute-start.5 = (bf16[256,512]{1,0:T(8,128)(2,1)S(1)}, bf16[256,512]{1,0:T(8,128)(2,1)S(1)}, u32[]{:S(2)}, u32[]{:S(2)}) collective-permute-start(bf16[256,512]{1,0:T(8,128)(2,1)S(1)} %fusion.42), channel_id=1, source_target_pairs={{0,1},{1,2},{2,3},{3,0},{4,5},{5,6},{6,7},{7,4},{8,9},{9,10},{10,1... | collective-permute-start | bytes 786440 | tf_op jit(solution)/shard_map/ppermute | solution.py:19
  282.6 10.9 %collective-permute-start.6 = (bf16[256,512]{1,0:T(8,128)(2,1)S(1)}, bf16[256,512]{1,0:T(8,128)(2,1)S(1)}, u32[]{:S(2)}, u32[]{:S(2)}) collective-permute-start(bf16[256,512]{1,0:T(8,128)(2,1)S(1)} %collective-permute-done.5), channel_id=1, source_target_pairs={{0,1},{1,2},{2,3},{3,0},{4,5},{5,6},{6,7},{7,4},{8,9},{9,10},{10,1... | collective-permute-start | bytes 786440 | tf_op jit(solution)/shard_map/ppermute | solution.py:19
  293.5 10.0 %collective-permute-start.7 = (bf16[256,512]{1,0:T(8,128)(2,1)S(1)}, bf16[256,512]{1,0:T(8,128)(2,1)S(1)}, u32[]{:S(2)}, u32[]{:S(2)}) collective-permute-start(bf16[256,512]{1,0:T(8,128)(2,1)S(1)} %collective-permute-done.6), channel_id=1, source_target_pairs={{0,1},{1,2},{2,3},{3,0},{4,5},{5,6},{6,7},{7,4},{8,9},{9,10},{10,1... | collective-permute-start | bytes 786440 | tf_op jit(solution)/shard_map/ppermute | solution.py:19
  332.8 2.7 copy-start.4
  337.9 2.1 collective-permute-start.8
  342.4 9.9 %collective-permute-start.9 = (bf16[256,512]{1,0:T(8,128)(2,1)S(1)}, bf16[256,512]{1,0:T(8,128)(2,1)S(1)}, u32[]{:S(2)}, u32[]{:S(2)}) collective-permute-start(bf16[256,512]{1,0:T(8,128)(2,1)S(1)} %fusion.49), channel_id=1, source_target_pairs={{0,1},{1,2},{2,3},{3,0},{4,5},{5,6},{6,7},{7,4},{8,9},{9,10},{10,1... | collective-permute-start | bytes 786440 | tf_op jit(solution)/shard_map/ppermute | solution.py:19
  352.3 11.0 %collective-permute-start.10 = (bf16[256,512]{1,0:T(8,128)(2,1)S(1)}, bf16[256,512]{1,0:T(8,128)(2,1)S(1)}, u32[]{:S(2)}, u32[]{:S(2)}) collective-permute-start(bf16[256,512]{1,0:T(8,128)(2,1)S(1)} %collective-permute-done.9), channel_id=1, source_target_pairs={{0,1},{1,2},{2,3},{3,0},{4,5},{5,6},{6,7},{7,4},{8,9},{9,10},{10,1... | collective-permute-start | bytes 786440 | tf_op jit(solution)/shard_map/ppermute | solution.py:19
  363.2 10.1 %collective-permute-start.11 = (bf16[256,512]{1,0:T(8,128)(2,1)S(1)}, bf16[256,512]{1,0:T(8,128)(2,1)S(1)}, u32[]{:S(2)}, u32[]{:S(2)}) collective-permute-start(bf16[256,512]{1,0:T(8,128)(2,1)S(1)} %collective-permute-done.10), channel_id=1, source_target_pairs={{0,1},{1,2},{2,3},{3,0},{4,5},{5,6},{6,7},{7,4},{8,9},{9,10},{10,1... | collective-permute-start | bytes 786440 | tf_op jit(solution)/shard_map/ppermute | solution.py:19
  373.4 11.7 %copy-start.2 = (f32[512]{0:T(512)S(1)}, f32[512]{0:T(512)}, u32[]{:S(2)}) copy-start(f32[512]{0:T(512)} %param.17) | copy-start | bytes 6148
Sparse Core Ops, SparseCore 0:
  9.2 30.7 all-gather.7
  41.6 45.7 all-gather.13
  88.9 46.3 all-gather.11
  136.7 46.3 all-gather.9
  184.5 46.3 all-gather.15
  234.9 28.0 all-gather.17
  307.6 25.1 all-gather.19
